TPU v7x, 128 devices: a whole 4x4x4 slice. The times are simulated.
128 devices in a mesh: dp: 4 (over x), kv: 16 (over z, y), tp: 2 (over core).
Axes of the slice: x: 4, y: 4, z: 4, core: 2. Of those that a mesh axis runs over, the one named last changes fastest.
Arguments:
- tokens: bfloat16 [32, 2048], P('dp', ('kv', 'tp')), may hold values from -30 to 30
- attention_gain: bfloat16 [2048], P(('kv', 'tp')), may hold values from 0.099609375 to 1.8984375
- query_one: bfloat16 [2048, 512], P('kv', 'tp'), may hold values from -0.125 to 0.125
- query_two: bfloat16 [2048, 512], P('kv', 'tp'), may hold values from -0.125 to 0.125
- key_one: bfloat16 [2048, 512], P('kv', 'tp'), may hold values from -2 to 2
- key_two: bfloat16 [2048, 512], P('kv', 'tp'), may hold values from -2 to 2
- value_weight: bfloat16 [2048, 1024], P('kv', 'tp'), may hold values from -0.125 to 0.125
- head_second_weight: float32 [8], P('tp'), may hold values from 0.3 to 0.8
- head_gain: float32 [128], replicated, may hold values from 0.1 to 1.9
- out_weight: bfloat16 [1024, 2048], P('tp', 'kv'), may hold values from -0.375 to 0.375
- mixer_gain: bfloat16 [2048], P(('kv', 'tp')), may hold values from 0.099609375 to 1.8984375
- gate_weight: bfloat16 [2048, 5632], P('kv', 'tp'), may hold values from -0.125 to 0.125
- up_weight: bfloat16 [2048, 5632], P('kv', 'tp'), may hold values from -0.125 to 0.125
- down_weight: bfloat16 [5632, 2048], P('tp', 'kv'), may hold values from -0.15625 to 0.15625
- key_cache: bfloat16 [32, 16384, 8, 128], P('dp', 'kv', 'tp'), may hold values from -240 to 240
- value_cache: bfloat16 [32, 16384, 8, 128], P('dp', 'kv', 'tp'), may hold values from -6 to 6
Outputs:
- layer_out: bfloat16 [32, 2048], P('dp', ('kv', 'tp'))
All inputs are finite; a program needn't handle non-finite values.
Results may differ from a plain program's by a relative error of at most 0.02.
Values may be sent and summed in bfloat16 or wider, within the bound.
A program may use at most 64 MiB of HBM per device.

v0:
```python
import jax
import jax.numpy as jnp
from jax import lax
from jax.sharding import Mesh
from jax.sharding import PartitionSpec as P

DH = 64
KV = ("kv_0", "kv_1")
KV_TP = ("kv_0", "kv_1", "tp")
NORM_EPSILON = 1e-06
HEAD_EPSILON = 1e-05
HEAD_SCALE = 0.8
ROTARY_BASE = 10000.0


def turned_gather(arrays, axis, dims):
    turned = [jnp.moveaxis(a, dim, 0) for a, dim in zip(arrays, dims)]
    both = jnp.concatenate([t.reshape(len(t), -1) for t in turned], axis=1)
    filled, at, done = (lax.all_gather(both, axis, axis=0, tiled=True), 0, [])
    for t, dim in zip(turned, dims):
        piece = filled[:, at : at + t[0].size].reshape(-1, *t.shape[1:])
        done.append(jnp.moveaxis(piece, 0, dim))
        at += t[0].size
    return tuple(done)


def copy_for_each(value, axis):
    copies = jnp.broadcast_to(value, (lax.axis_size(axis), *value.shape))
    return lax.all_to_all(copies, axis, split_axis=0, concat_axis=0, tiled=True)


def of_everyone(value, axis):
    everything = copy_for_each(value, axis)
    return jnp.sum(everything, axis=0)


def in_one(arrays, axis):
    line, at, done = (jnp.concatenate([a.reshape(-1) for a in arrays]), 0, [])
    subtotal = of_everyone(line, axis)
    for a in arrays:
        done.append(subtotal[at : at + a.size].reshape(a.shape))
        at += a.size
    return tuple(done)


def collected_together(value, axis):
    leaves = jax.tree.leaves(value)
    turns = sorted(range(len(leaves)), key=lambda k: -leaves[k].size)
    width = (1, *leaves[turns[0]].shape)[-1]
    lines = [
        jnp.pad(leaves[k].reshape(-1), (0, -leaves[k].size % width)).reshape(-1, width)
        for k in turns
    ]
    both, at, found = (lax.all_gather(jnp.concatenate(lines), axis), 0, {})
    for k, line in zip(turns, lines):
        piece = both[:, at : at + len(line)].reshape(len(both), -1)
        found[k] = piece[:, : leaves[k].size].reshape(-1, *leaves[k].shape)
        at += len(line)
    numbers = iter(range(len(leaves)))
    return jax.tree.map(lambda _: found[next(numbers)], value)


def joined_all(value, axes, combine):
    for axis in axes:
        pieces = collected_together(value, axis)
        value = jax.tree.map(lambda part: part[0], pieces)
        for k in range(1, lax.axis_size(axis)):
            value = combine(value, jax.tree.map(lambda part: part[k], pieces))
    return value


def split_up(value, dim, devices):
    before, after = (value.shape[:dim], value.shape[dim + 1 :])
    return jnp.moveaxis(value.reshape(*before, devices, -1, *after), dim, 0)


def sent_and_summed(value, axis, dim):
    parts = split_up(value, dim, lax.axis_size(axis))
    arrived = lax.all_to_all(parts, axis, split_axis=0, concat_axis=0, tiled=True)
    return arrived.astype(jnp.float32).sum(axis=0)


def sent_and_summed_2(value, axis, dim):
    devices = lax.axis_size(axis)
    parts = lax.all_to_all(split_up(value, dim, devices), axis, 0, 0, tiled=True)
    return jnp.sum(parts, axis=0)


def in_one_piece(arrays, axis, dim, along):
    both = jnp.concatenate(arrays, axis=along)
    filled, at, done = (sent_and_summed_2(both, axis, dim), 0, [])
    for a in arrays:
        done.append(lax.slice_in_dim(filled, at, at + a.shape[along], axis=along))
        at += a.shape[along]
    return tuple(done)


def laid_out(parts, dim):
    shape = list(parts.shape[1:])
    shape[dim] *= parts.shape[0]
    return jnp.moveaxis(parts, 0, dim).reshape(shape)


def gathered_copies(value, axis, dim):
    parts = copy_for_each(value, axis)
    return laid_out(parts, dim)


def rotate(vectors, position):
    half_width = vectors.shape[-1] // 2
    frequency = 1.0 / ROTARY_BASE ** (jnp.arange(half_width, dtype=jnp.float32) / half_width)
    angles = position * frequency
    cosine = jnp.cos(angles)
    sine_value = jnp.sin(angles)
    lead_half = vectors[..., :half_width]
    tail_half = vectors[..., half_width:]
    return jnp.concatenate(
        [lead_half * cosine - tail_half * sine_value, tail_half * cosine + lead_half * sine_value],
        axis=-1,
    )


def combine(earlier, later):
    peak_left, total_left, weighted_left = earlier
    peak_right, total_right, weighted_right = later
    peak_score = jnp.maximum(peak_left, peak_right)
    factor_left = jnp.exp(peak_left - peak_score)
    factor_right = jnp.exp(peak_right - peak_score)
    return (
        peak_score,
        total_left * factor_left + total_right * factor_right,
        weighted_left * factor_left[..., None] + weighted_right * factor_right[..., None],
    )


def shards(
    tokens,
    attention_gain,
    query_one,
    query_two,
    key_one,
    key_two,
    value_weight,
    head_second_weight,
    head_gain,
    out_weight,
    mixer_gain,
    gate_weight,
    up_weight,
    down_weight,
    key_cache,
    value_cache,
):
    row_count = tokens.shape[0]
    position_group = lax.axis_size(KV)
    model_width = tokens.shape[1] * position_group * lax.axis_size("tp")
    local_heads = query_one.shape[1] // DH
    local_positions = key_cache.shape[1]
    position = jnp.float32(local_positions * position_group)
    score_scale = DH ** (-0.5)
    token_values = tokens.astype(jnp.float32)
    row_block, gain_block = turned_gather((tokens, attention_gain), "tp", (1, 0))
    block_values = row_block.astype(jnp.float32)
    scaled = (block_values * gain_block.astype(jnp.float32)).astype(jnp.bfloat16)
    query_first = jnp.dot(scaled, query_one, preferred_element_type=jnp.float32)
    query_second = jnp.dot(scaled, query_two, preferred_element_type=jnp.float32)
    key_first = jnp.dot(scaled, key_one, preferred_element_type=jnp.float32)
    key_second = jnp.dot(scaled, key_two, preferred_element_type=jnp.float32)
    value_part = jnp.dot(scaled, value_weight, preferred_element_type=jnp.float32)
    block_square = jnp.sum(block_values * block_values, axis=1)
    query_first, query_second, key_first, key_second, value_part, square_total = in_one(
        (query_first, query_second, key_first, key_second, value_part, block_square), KV
    )
    row_ratio = lax.rsqrt(square_total / model_width + NORM_EPSILON)[:, None]

    def paired(lead_part, tail_part):
        both = jnp.stack(
            [
                (lead_part * row_ratio).reshape(row_count, local_heads, DH),
                (tail_part * row_ratio).reshape(row_count, local_heads, DH),
            ],
            axis=2,
        )
        return rotate(both, position).astype(jnp.bfloat16)

    queries = paired(query_first, query_second)
    new_keys = paired(key_first, key_second)
    new_values = (
        (value_part * row_ratio).astype(jnp.bfloat16).reshape(row_count, local_heads, 2 * DH)
    )
    zero_half = jnp.zeros((row_count, local_heads, DH), jnp.bfloat16)
    padded_query_rows = jnp.stack(
        [
            jnp.concatenate([queries[:, :, 0], zero_half], axis=-1),
            jnp.concatenate([zero_half, queries[:, :, 1]], axis=-1),
        ],
        axis=2,
    )
    logit_scores = (
        jnp.einsum(
            "bhmk,bphk->bhmp", padded_query_rows, key_cache, preferred_element_type=jnp.float32
        )
        * score_scale
    )
    peak_score = jnp.max(logit_scores, axis=-1)
    exponent = jnp.exp(logit_scores - peak_score[..., None])
    weight_sum = jnp.sum(exponent, axis=-1)
    weighted = jnp.einsum(
        "bhmp,bphe->bhme",
        exponent.astype(jnp.bfloat16),
        value_cache,
        preferred_element_type=jnp.float32,
    )
    peak_score, weight_sum, weighted = joined_all((peak_score, weight_sum, weighted), KV, combine)
    own_score = (
        jnp.sum(queries.astype(jnp.float32) * new_keys.astype(jnp.float32), axis=-1) * score_scale
    )
    final_peak = jnp.maximum(peak_score, own_score)
    cache_factor = jnp.exp(peak_score - final_peak)
    own_weight = jnp.exp(own_score - final_peak)
    weight_sum = weight_sum * cache_factor + own_weight
    weighted = (
        weighted * cache_factor[..., None]
        + own_weight[..., None] * new_values.astype(jnp.float32)[:, :, None, :]
    )
    averaged = weighted / weight_sum[..., None]
    difference = averaged[:, :, 0] - head_second_weight[None, :, None] * averaged[:, :, 1]
    inverse_norm = lax.rsqrt(
        jnp.mean(difference * difference, axis=-1, keepdims=True) + HEAD_EPSILON
    )
    attended = (difference * inverse_norm * head_gain[None, None, :] * HEAD_SCALE).astype(
        jnp.bfloat16
    )
    attended = attended.reshape(row_count, local_heads * 2 * DH)
    attention_term = jnp.dot(attended, out_weight, preferred_element_type=jnp.float32)
    attention_out = sent_and_summed(attention_term.astype(jnp.bfloat16), "tp", 1)
    mixed = (token_values + attention_out).astype(jnp.bfloat16)
    mixed_values = mixed.astype(jnp.float32)
    mixer_block, mixer_gain_block = turned_gather((mixed, mixer_gain), "tp", (1, 0))
    mixer_block_values = mixer_block.astype(jnp.float32)
    mixer_scaled = (mixer_block_values * mixer_gain_block.astype(jnp.float32)).astype(jnp.bfloat16)
    gate_part = jnp.dot(mixer_scaled, gate_weight, preferred_element_type=jnp.float32)
    up_part = jnp.dot(mixer_scaled, up_weight, preferred_element_type=jnp.float32)
    mixer_square = jnp.sum(mixer_block_values * mixer_block_values, axis=1)
    square_columns = jnp.broadcast_to(mixer_square[:, None], (row_count, position_group))
    gate_sum, up_sum, total_column = (
        *in_one_piece((gate_part, up_part), KV, 1, 0),
        sent_and_summed_2(square_columns, KV, 1),
    )
    mixer_total = total_column[:, 0]
    mixer_ratio = lax.rsqrt(mixer_total / model_width + NORM_EPSILON)[:, None]
    hidden_share = (jax.nn.silu(gate_sum * mixer_ratio) * (up_sum * mixer_ratio)).astype(
        jnp.bfloat16
    )
    hidden_state = gathered_copies(hidden_share, KV, 1)
    mixer_term = jnp.dot(hidden_state, down_weight, preferred_element_type=jnp.float32)
    mixer_out = sent_and_summed(mixer_term.astype(jnp.bfloat16), "tp", 1)
    return (mixed_values + mixer_out).astype(jnp.bfloat16)


def solution(mesh):
    torus = Mesh(
        mesh.devices.reshape(mesh.shape["dp"], 4, 4, mesh.shape["tp"]), ("dp", "kv_0", "kv_1", "tp")
    )
    return jax.shard_map(
        shards,
        mesh=torus,
        in_specs=(
            P("dp", KV_TP),
            P(KV_TP),
            P(KV, "tp"),
            P(KV, "tp"),
            P(KV, "tp"),
            P(KV, "tp"),
            P(KV, "tp"),
            P("tp"),
            P(),
            P("tp", KV),
            P(KV_TP),
            P(KV, "tp"),
            P(KV, "tp"),
            P("tp", KV),
            P("dp", KV, "tp", None),
            P("dp", KV, "tp", None),
        ),
        out_specs=P("dp", KV_TP),
        check_vma=False,
    )
```

profile of v0, /device:TPU:1, one launch (start us, length us, event | category | flops | bytes accessed | tf_op | source)
XLA Modules:
  0.0 119.3 jit_solution(6227983753720261710)
XLA Ops:
  0.0 0.8 maximum_bitcast_fusion.2
  0.8 2.8 %all-gather.2 = bf16[2,64,9]{1,2,0:T(8,128)(2,1)S(1)} all-gather(bf16[1,64,9]{1,2,0:T(8,128)(2,1)S(1)} %maximum_bitcast_fusion.2), channel_id=1, replica_groups=mesh['dp'=4,'kv_0'=4,'kv_1'=4,'tp'=2] {'tp'}, dimensions={0}, use_global_device_ids=true | all-gather | bytes 3456 | tf_op jit(solution)/shard_map/all_gather | solution.py:19
  3.8 1.0 convolution_bitcast_fusion.4
  4.8 1.0 convolution_bitcast_fusion.3
  5.8 1.0 convolution_bitcast_fusion.2
  6.8 1.0 convolution_bitcast_fusion.1
  7.8 1.0 convolution_bitcast_fusion
  8.8 1.3 %broadcast_in_dim.4 = f32[16,1,12296]{2,1,0:T(1,128)} broadcast(f32[12296]{0:T(1024)S(1)} %constant_dynamic-update-slice_fusion), dimensions={2} | broadcast | bytes 836128 | tf_op jit(solution)/shard_map/broadcast_in_dim | solution.py:28
  10.1 7.9 %all-to-all-start = ((f32[16,1,12296]{2,1,0:T(1,128)}), f32[16,1,12296]{2,1,0:T(1,128)S(1)}, u32[]{:S(2)}, u32[]{:S(2)}) async-start(f32[16,1,12296]{2,1,0:T(1,128)} %broadcast_in_dim.4), calls=%async_computation | async-start | bytes 1589248 | tf_op jit(solution)/shard_map/all_to_all | solution.py:29
  18.1 0.7 broadcast_bitcast_fusion
  18.8 12.8 %all-to-all-done = f32[16,1,12296]{2,1,0:T(1,128)S(1)} async-done(((f32[16,1,12296]{2,1,0:T(1,128)}), f32[16,1,12296]{2,1,0:T(1,128)S(1)}, u32[]{:S(2)}, u32[]{:S(2)}) %all-to-all-start) | async-done | bytes 786976 | tf_op jit(solution)/shard_map/all_to_all | solution.py:29
  32.9 5.7 %fusion.94 = (f32[8,4,2]{2,1,0:T(4,128)S(1)}, f32[8,4,2,1024]{3,2,1,0:T(2,128)S(1)}) fusion(bf16[8,1024,4,128]{3,2,1,0:T(4,128)(2,1)} %param.30, bf16[8,4,1,128]{3,2,1,0:T(2,128)(2,1)S(1)} %copy.107, bf16[8,4,1,128]{3,2,1,0:T(2,128)(2,1)S(1)} %copy.106), kind=kOutput, calls=%fused_computation.184 | convolution fusion | flops 16940992 | bytes 8667392 | tf_op jit(solution)/shard_map/bhmk,bphk->bhmp/dot_general | solution.py:200
  39.2 4.9 %fusion = f32[8,4,2,128]{3,2,1,0:T(2,128)S(1)} fusion(bf16[8,1024,4,128]{3,2,1,0:T(4,128)(2,1)} %param.31, f32[8,4,2,1024]{3,2,1,0:T(2,128)S(1)} %get-tuple-element.57, f32[8,4,2]{2,1,0:T(4,128)S(1)} %get-tuple-element.56), kind=kOutput, calls=%fused_computation | convolution fusion | flops 16908288 | bytes 8683776 | tf_op jit(solution)/shard_map/bhmp,bphe->bhme/dot_general | solution.py:208
  44.3 9.6 %all-gather.3 = f32[4,66,128]{2,1,0:T(8,128)S(1)} all-gather(f32[1,66,128]{2,1,0:T(8,128)S(1)} %maximum_bitcast_fusion), channel_id=2, replica_groups=mesh['dp'=4,'kv_0'=4,'kv_1'=4,'tp'=2] {'kv_0'}, dimensions={0}, use_global_device_ids=true | all-gather | bytes 168960 | tf_op jit(solution)/shard_map/all_gather | solution.py:54
  54.0 9.6 %all-gather.4 = f32[4,66,128]{2,1,0:T(8,128)S(1)} all-gather(f32[1,66,128]{2,1,0:T(8,128)S(1)} %maximum_bitcast_fusion.1), channel_id=3, replica_groups=mesh['dp'=4,'kv_0'=4,'kv_1'=4,'tp'=2] {'kv_1'}, dimensions={0}, use_global_device_ids=true | all-gather | bytes 168960 | tf_op jit(solution)/shard_map/all_gather | solution.py:54
  67.0 10.2 %all_to_all.31 = bf16[2,2,256]{2,1,0:T(2,128)(2,1)S(1)} all-to-all(bf16[2,2,256]{2,1,0:T(2,128)(2,1)S(1)} %reshape.630), channel_id=1, replica_groups=mesh['dp'=4,'kv_0'=4,'kv_1'=4,'tp'=2] {'tp'}, dimensions={0} | all-to-all | bytes 4096 | tf_op jit(solution)/shard_map/all_to_all | solution.py:79
  77.3 1.8 %all-gather.5 = bf16[2,64,9]{1,2,0:T(8,128)(2,1)S(1)} all-gather(bf16[1,64,9]{1,2,0:T(8,128)(2,1)S(1)} %maximum_bitcast_fusion.3), channel_id=1, replica_groups=mesh['dp'=4,'kv_0'=4,'kv_1'=4,'tp'=2] {'tp'}, dimensions={0}, use_global_device_ids=true | all-gather | bytes 3456 | tf_op jit(solution)/shard_map/all_gather | solution.py:19
  80.3 3.5 %all-to-all-start.3 = ((f32[16,8,1]{1,2,0:T(1,128)}), f32[16,8,1]{1,2,0:T(1,128)S(1)}, u32[]{:S(2)}, u32[]{:S(2)}) async-start(f32[16,8,1]{1,2,0:T(1,128)} %transpose.84), calls=%async_computation.3 | async-start | bytes 16384 | tf_op jit(solution)/shard_map/all_to_all | solution.py:85
  84.1 0.8 copy.191
  84.9 5.3 %all-to-all-done.3 = f32[16,8,1]{1,2,0:T(1,128)S(1)} async-done(((f32[16,8,1]{1,2,0:T(1,128)}), f32[16,8,1]{1,2,0:T(1,128)S(1)}, u32[]{:S(2)}, u32[]{:S(2)}) %all-to-all-start.3) | async-done | bytes 544 | tf_op jit(solution)/shard_map/all_to_all | solution.py:85
  90.3 3.5 %all-to-all-start.2 = ((f32[16,16,176]{2,1,0:T(8,128)}), f32[16,16,176]{2,1,0:T(8,128)S(1)}, u32[]{:S(2)}, u32[]{:S(2)}) async-start(f32[16,16,176]{2,1,0:T(8,128)} %bitcast.218), calls=%async_computation.2 | async-start | bytes 524288 | tf_op jit(solution)/shard_map/all_to_all | solution.py:85
  93.8 7.5 %all-to-all-done.2 = f32[16,16,176]{2,1,0:T(8,128)S(1)} async-done(((f32[16,16,176]{2,1,0:T(8,128)}), f32[16,16,176]{2,1,0:T(8,128)S(1)}, u32[]{:S(2)}, u32[]{:S(2)}) %all-to-all-start.2) | async-done | bytes 180256 | tf_op jit(solution)/shard_map/all_to_all | solution.py:85
  101.5 9.4 %all_to_all.32 = bf16[16,8,176]{2,1,0:T(8,128)(2,1)S(1)} all-to-all(bf16[16,8,176]{2,1,0:T(8,128)(2,1)S(1)} %broadcast_in_dim.5), channel_id=1, replica_groups=mesh['dp'=4,'kv_0'=4,'kv_1'=4,'tp'=2] {'kv_0','kv_1'}, dimensions={0} | all-to-all | bytes 90112 | tf_op jit(solution)/shard_map/all_to_all | solution.py:29
  111.4 7.3 %all_to_all.33 = bf16[2,2,256]{2,1,0:T(2,128)(2,1)S(1)} all-to-all(bf16[2,2,256]{2,1,0:T(2,128)(2,1)S(1)} %reshape.632), channel_id=1, replica_groups=mesh['dp'=4,'kv_0'=4,'kv_1'=4,'tp'=2] {'tp'}, dimensions={0} | all-to-all | bytes 4096 | tf_op jit(solution)/shard_map/all_to_all | solution.py:79
  (116 shorter events, 8.5 us)
Async XLA Ops:
  0.0 79.3 %copy-start = (bf16[128,2816]{1,0:T(8,128)(2,1)S(1)}, bf16[128,2816]{1,0:T(8,128)(2,1)}, u32[]{:S(2)}) copy-start(bf16[128,2816]{1,0:T(8,128)(2,1)} %param.27) | copy-start | bytes 2162692
  10.1 21.5 %all-to-all-start = ((f32[16,1,12296]{2,1,0:T(1,128)}), f32[16,1,12296]{2,1,0:T(1,128)S(1)}, u32[]{:S(2)}, u32[]{:S(2)}) async-start(f32[16,1,12296]{2,1,0:T(1,128)} %broadcast_in_dim.4), calls=%async_computation | async-start | bytes 1589248 | tf_op jit(solution)/shard_map/all_to_all | solution.py:29
  39.1 27.2 %copy-start.4 = (f32[4]{0:T(128)S(1)}, f32[4]{0:T(128)}, u32[]{:S(2)}) copy-start(f32[4]{0:T(128)} %param.23) | copy-start | bytes 52
  39.1 27.5 %copy-start.6 = (bf16[512,128]{1,0:T(8,128)(2,1)S(1)}, bf16[512,128]{1,0:T(8,128)(2,1)}, u32[]{:S(2)}) copy-start(bf16[512,128]{1,0:T(8,128)(2,1)} %param.25) | copy-start | bytes 393220
  39.2 38.1 %copy-start.3 = (bf16[8,64]{1,0:T(8,128)(2,1)S(1)}, bf16[8,64]{1,0:T(8,128)(2,1)}, u32[]{:S(2)}) copy-start(bf16[8,64]{1,0:T(8,128)(2,1)} %param.16) | copy-start | bytes 3076
  39.2 38.1 %copy-start.5 = (bf16[64]{0:T(256)(128)(2,1)S(1)}, bf16[64]{0:T(256)(128)(2,1)}, u32[]{:S(2)}) copy-start(bf16[64]{0:T(256)(128)(2,1)} %param.26) | copy-start | bytes 388
  39.2 40.3 %copy-start.1 = (bf16[128,2816]{1,0:T(8,128)(2,1)S(1)}, bf16[128,2816]{1,0:T(8,128)(2,1)}, u32[]{:S(2)}) copy-start(bf16[128,2816]{1,0:T(8,128)(2,1)} %param.28) | copy-start | bytes 2162692
  39.2 71.8 %copy-start.2 = (bf16[2816,128]{1,0:T(8,128)(2,1)S(1)}, bf16[2816,128]{1,0:T(8,128)(2,1)}, u32[]{:S(2)}) copy-start(bf16[2816,128]{1,0:T(8,128)(2,1)} %param.29) | copy-start | bytes 2162692
  80.3 9.9 %all-to-all-start.3 = ((f32[16,8,1]{1,2,0:T(1,128)}), f32[16,8,1]{1,2,0:T(1,128)S(1)}, u32[]{:S(2)}, u32[]{:S(2)}) async-start(f32[16,8,1]{1,2,0:T(1,128)} %transpose.84), calls=%async_computation.3 | async-start | bytes 16384 | tf_op jit(solution)/shard_map/all_to_all | solution.py:85
  90.3 11.1 %all-to-all-start.2 = ((f32[16,16,176]{2,1,0:T(8,128)}), f32[16,16,176]{2,1,0:T(8,128)S(1)}, u32[]{:S(2)}, u32[]{:S(2)}) async-start(f32[16,16,176]{2,1,0:T(8,128)} %bitcast.218), calls=%async_computation.2 | async-start | bytes 524288 | tf_op jit(solution)/shard_map/all_to_all | solution.py:85
where the time goes:
time: 120 us; the launch traced here: 119 us
  blocking collectives  50.7 us (42%)
  waiting for transfers between devices  25.7 us (21%)
  matrix products  16.4 us (14%)
  starting transfers between devices  14.9 us (12%)
  local copies, waits for them, and re-layouts  7.53 us (6%)
  other arithmetic  3.79 us (3%)
    all_gather x2, blocking collectives, collected_together(): both, at, found = (lax.all_gather(jnp.concatenate(lines), axis), 0, {})  19.2 us
    all_to_all x2, blocking collectives, sent_and_summed(): lax.all_to_all(parts, axis, split_axis=0, concat_axis=0, tiled=True)  17.4 us
    all_to_all x1, waiting for transfers between devices, copy_for_each(): return lax.all_to_all(copies, axis, split_axis=0, concat_axis=0, tiled=True)  12.8 us
    all_to_all x2, waiting for transfers between devices, sent_and_summed_2(): lax.all_to_all(split_up(value, dim, devices), axis, 0, 0, tiled=True)  12.8 us
    all_to_all x1, blocking collectives, copy_for_each(): return lax.all_to_all(copies, axis, split_axis=0, concat_axis=0, tiled=True)  9.4 us
    all_to_all x1, starting transfers between devices, copy_for_each(): return lax.all_to_all(copies, axis, split_axis=0, concat_axis=0, tiled=True)  7.88 us
    all_to_all x2, starting transfers between devices, sent_and_summed_2(): lax.all_to_all(split_up(value, dim, devices), axis, 0, 0, tiled=True)  7.01 us
    dot_general x1, matrix products, shards(): jnp.einsum('bhmk,bphk->bhmp', padded_query_rows, key_cache, preferred_ele...  5.74 us
  transfers between devices with their start and end apart: 3, of which 3 were waited for; matrix products, arithmetic and copies ran while one was open for 2% of the time, Pallas kernels for 0%

commit v1 on v0

--- a/solution.py
+++ b/solution.py
@@ -16,7 +16,13 @@
 def turned_gather(arrays, axis, dims):
     turned = [jnp.moveaxis(a, dim, 0) for a, dim in zip(arrays, dims)]
     both = jnp.concatenate([t.reshape(len(t), -1) for t in turned], axis=1)
-    filled, at, done = (lax.all_gather(both, axis, axis=0, tiled=True), 0, [])
+    filled, at, done = (
+        jnp.concatenate(
+            lax.all_to_all(jnp.stack([both] * lax.axis_size(axis)), axis, 0, 0), axis=0
+        ),
+        0,
+        [],
+    )
     for t, dim in zip(turned, dims):
         piece = filled[:, at : at + t[0].size].reshape(-1, *t.shape[1:])
         done.append(jnp.moveaxis(piece, 0, dim))

time: 120 us -> 124 us (1.033)
  blocking collectives: 50.7 us -> 54.4 us
    all_to_all x0 -> x2, blocking collectives: none -> 8.42 us  [turned_gather(): lax.all_to_all(jnp.stack([both] * lax.axis_size(axis)), axis, 0, 0)]
    all_gather x2 -> x0, blocking collectives: 4.66 us -> none  [turned_gather(): filled, at, done = (lax.all_gather(both, axis, axis=0, tiled=True), 0, [])]
where the time goes in v1:
time: 124 us; the launch traced here: 123 us
  blocking collectives  54.4 us (44%)
  waiting for transfers between devices  25.7 us (21%)
  matrix products  16.4 us (13%)
  starting transfers between devices  14.9 us (12%)
  local copies, waits for them, and re-layouts  7.89 us (6%)
  other arithmetic  3.81 us (3%)
    all_gather x2, blocking collectives, collected_together(): both, at, found = (lax.all_gather(jnp.concatenate(lines), axis), 0, {})  19.2 us
    all_to_all x2, blocking collectives, sent_and_summed(): lax.all_to_all(parts, axis, split_axis=0, concat_axis=0, tiled=True)  17.4 us
    all_to_all x1, waiting for transfers between devices, copy_for_each(): return lax.all_to_all(copies, axis, split_axis=0, concat_axis=0, tiled=True)  12.9 us
    all_to_all x2, waiting for transfers between devices, sent_and_summed_2(): lax.all_to_all(split_up(value, dim, devices), axis, 0, 0, tiled=True)  12.8 us
    all_to_all x1, blocking collectives, copy_for_each(): return lax.all_to_all(copies, axis, split_axis=0, concat_axis=0, tiled=True)  9.39 us
    all_to_all x2, blocking collectives, turned_gather(): lax.all_to_all(jnp.stack([both] * lax.axis_size(axis)), axis, 0, 0)  8.42 us
    all_to_all x1, starting transfers between devices, copy_for_each(): return lax.all_to_all(copies, axis, split_axis=0, concat_axis=0, tiled=True)  7.88 us
    all_to_all x2, starting transfers between devices, sent_and_summed_2(): lax.all_to_all(split_up(value, dim, devices), axis, 0, 0, tiled=True)  7.01 us
  transfers between devices with their start and end apart: 3, of which 3 were waited for; matrix products, arithmetic and copies ran while one was open for 2% of the time, Pallas kernels for 0%

profile of v1, /device:TPU:1, one launch (start us, length us, event | category | flops | bytes accessed | tf_op | source)
XLA Modules:
  0.0 123.5 jit_solution(14772903415737908162)
XLA Ops:
  0.0 0.8 maximum_bitcast_fusion.2
  0.9 4.7 %all_to_all.41 = bf16[2,2,288]{2,1,0:T(2,128)(2,1)S(1)} all-to-all(bf16[2,2,288]{2,1,0:T(2,128)(2,1)S(1)} %reshape.634), channel_id=1, replica_groups=mesh['dp'=4,'kv_0'=4,'kv_1'=4,'tp'=2] {'tp'}, dimensions={0} | all-to-all | bytes 4608 | tf_op jit(solution)/shard_map/all_to_all | solution.py:21
  5.9 1.0 convolution_bitcast_fusion.4
  6.9 1.0 convolution_bitcast_fusion.3
  7.9 1.0 convolution_bitcast_fusion.2
  8.9 1.0 convolution_bitcast_fusion.1
  9.8 1.0 convolution_bitcast_fusion
  10.9 1.3 %broadcast_in_dim.4 = f32[16,1,12296]{2,1,0:T(1,128)} broadcast(f32[12296]{0:T(1024)S(1)} %constant_dynamic-update-slice_fusion), dimensions={2} | broadcast | bytes 836128 | tf_op jit(solution)/shard_map/broadcast_in_dim | solution.py:34
  12.2 7.9 %all-to-all-start.1 = ((f32[16,1,12296]{2,1,0:T(1,128)}), f32[16,1,12296]{2,1,0:T(1,128)S(1)}, u32[]{:S(2)}, u32[]{:S(2)}) async-start(f32[16,1,12296]{2,1,0:T(1,128)} %broadcast_in_dim.4), calls=%async_computation.1 | async-start | bytes 1589248 | tf_op jit(solution)/shard_map/all_to_all | solution.py:35
  20.2 0.7 broadcast_bitcast_fusion
  20.9 12.9 %all-to-all-done.1 = f32[16,1,12296]{2,1,0:T(1,128)S(1)} async-done(((f32[16,1,12296]{2,1,0:T(1,128)}), f32[16,1,12296]{2,1,0:T(1,128)S(1)}, u32[]{:S(2)}, u32[]{:S(2)}) %all-to-all-start.1) | async-done | bytes 786976 | tf_op jit(solution)/shard_map/all_to_all | solution.py:35
  35.0 5.7 %fusion.94 = (f32[8,4,2]{2,1,0:T(4,128)S(1)}, f32[8,4,2,1024]{3,2,1,0:T(2,128)S(1)}) fusion(bf16[8,1024,4,128]{3,2,1,0:T(4,128)(2,1)} %param.30, bf16[8,4,1,128]{3,2,1,0:T(2,128)(2,1)S(1)} %copy.107, bf16[8,4,1,128]{3,2,1,0:T(2,128)(2,1)S(1)} %copy.106), kind=kOutput, calls=%fused_computation.186 | convolution fusion | flops 16940992 | bytes 8667392 | tf_op jit(solution)/shard_map/bhmk,bphk->bhmp/dot_general | solution.py:206
  41.3 4.9 %fusion = f32[8,4,2,128]{3,2,1,0:T(2,128)S(1)} fusion(bf16[8,1024,4,128]{3,2,1,0:T(4,128)(2,1)} %param.31, f32[8,4,2,1024]{3,2,1,0:T(2,128)S(1)} %get-tuple-element.57, f32[8,4,2]{2,1,0:T(4,128)S(1)} %get-tuple-element.56), kind=kOutput, calls=%fused_computation | convolution fusion | flops 16908288 | bytes 8683776 | tf_op jit(solution)/shard_map/bhmp,bphe->bhme/dot_general | solution.py:214
  46.4 9.5 %all-gather.2 = f32[4,66,128]{2,1,0:T(8,128)S(1)} all-gather(f32[1,66,128]{2,1,0:T(8,128)S(1)} %maximum_bitcast_fusion), channel_id=2, replica_groups=mesh['dp'=4,'kv_0'=4,'kv_1'=4,'tp'=2] {'kv_0'}, dimensions={0}, use_global_device_ids=true | all-gather | bytes 168960 | tf_op jit(solution)/shard_map/all_gather | solution.py:60
  56.1 9.6 %all-gather.3 = f32[4,66,128]{2,1,0:T(8,128)S(1)} all-gather(f32[1,66,128]{2,1,0:T(8,128)S(1)} %maximum_bitcast_fusion.1), channel_id=3, replica_groups=mesh['dp'=4,'kv_0'=4,'kv_1'=4,'tp'=2] {'kv_1'}, dimensions={0}, use_global_device_ids=true | all-gather | bytes 168960 | tf_op jit(solution)/shard_map/all_gather | solution.py:60
  69.1 10.2 %all_to_all.42 = bf16[2,2,256]{2,1,0:T(2,128)(2,1)S(1)} all-to-all(bf16[2,2,256]{2,1,0:T(2,128)(2,1)S(1)} %reshape.636), channel_id=1, replica_groups=mesh['dp'=4,'kv_0'=4,'kv_1'=4,'tp'=2] {'tp'}, dimensions={0} | all-to-all | bytes 4096 | tf_op jit(solution)/shard_map/all_to_all | solution.py:85
  79.5 3.7 %all_to_all.43 = bf16[2,2,288]{2,1,0:T(2,128)(2,1)S(1)} all-to-all(bf16[2,2,288]{2,1,0:T(2,128)(2,1)S(1)} %reshape.638), channel_id=1, replica_groups=mesh['dp'=4,'kv_0'=4,'kv_1'=4,'tp'=2] {'tp'}, dimensions={0} | all-to-all | bytes 4608 | tf_op jit(solution)/shard_map/all_to_all | solution.py:21
  84.5 3.5 %all-to-all-start.5 = ((f32[16,8,1]{1,2,0:T(1,128)}), f32[16,8,1]{1,2,0:T(1,128)S(1)}, u32[]{:S(2)}, u32[]{:S(2)}) async-start(f32[16,8,1]{1,2,0:T(1,128)} %transpose.84), calls=%async_computation.5 | async-start | bytes 16384 | tf_op jit(solution)/shard_map/all_to_all | solution.py:91
  88.2 0.8 copy.191
  89.1 5.3 %all-to-all-done.5 = f32[16,8,1]{1,2,0:T(1,128)S(1)} async-done(((f32[16,8,1]{1,2,0:T(1,128)}), f32[16,8,1]{1,2,0:T(1,128)S(1)}, u32[]{:S(2)}, u32[]{:S(2)}) %all-to-all-start.5) | async-done | bytes 544 | tf_op jit(solution)/shard_map/all_to_all | solution.py:91
  94.4 3.5 %all-to-all-start.4 = ((f32[16,16,176]{2,1,0:T(8,128)}), f32[16,16,176]{2,1,0:T(8,128)S(1)}, u32[]{:S(2)}, u32[]{:S(2)}) async-start(f32[16,16,176]{2,1,0:T(8,128)} %bitcast.224), calls=%async_computation.4 | async-start | bytes 524288 | tf_op jit(solution)/shard_map/all_to_all | solution.py:91
  98.0 7.5 %all-to-all-done.4 = f32[16,16,176]{2,1,0:T(8,128)S(1)} async-done(((f32[16,16,176]{2,1,0:T(8,128)}), f32[16,16,176]{2,1,0:T(8,128)S(1)}, u32[]{:S(2)}, u32[]{:S(2)}) %all-to-all-start.4) | async-done | bytes 180256 | tf_op jit(solution)/shard_map/all_to_all | solution.py:91
  105.6 9.4 %all_to_all.44 = bf16[16,8,176]{2,1,0:T(8,128)(2,1)S(1)} all-to-all(bf16[16,8,176]{2,1,0:T(8,128)(2,1)S(1)} %broadcast_in_dim.5), channel_id=1, replica_groups=mesh['dp'=4,'kv_0'=4,'kv_1'=4,'tp'=2] {'kv_0','kv_1'}, dimensions={0} | all-to-all | bytes 90112 | tf_op jit(solution)/shard_map/all_to_all | solution.py:35
  115.6 7.3 %all_to_all.45 = bf16[2,2,256]{2,1,0:T(2,128)(2,1)S(1)} all-to-all(bf16[2,2,256]{2,1,0:T(2,128)(2,1)S(1)} %reshape.640), channel_id=1, replica_groups=mesh['dp'=4,'kv_0'=4,'kv_1'=4,'tp'=2] {'tp'}, dimensions={0} | all-to-all | bytes 4096 | tf_op jit(solution)/shard_map/all_to_all | solution.py:85
  (122 shorter events, 8.9 us)
Async XLA Ops:
  0.0 83.5 %copy-start = (bf16[128,2816]{1,0:T(8,128)(2,1)S(1)}, bf16[128,2816]{1,0:T(8,128)(2,1)}, u32[]{:S(2)}) copy-start(bf16[128,2816]{1,0:T(8,128)(2,1)} %param.27) | copy-start | bytes 2162692
  12.2 21.5 %all-to-all-start.1 = ((f32[16,1,12296]{2,1,0:T(1,128)}), f32[16,1,12296]{2,1,0:T(1,128)S(1)}, u32[]{:S(2)}, u32[]{:S(2)}) async-start(f32[16,1,12296]{2,1,0:T(1,128)} %broadcast_in_dim.4), calls=%async_computation.1 | async-start | bytes 1589248 | tf_op jit(solution)/shard_map/all_to_all | solution.py:35
  41.2 27.2 %copy-start.4 = (f32[4]{0:T(128)S(1)}, f32[4]{0:T(128)}, u32[]{:S(2)}) copy-start(f32[4]{0:T(128)} %param.23) | copy-start | bytes 52
  41.2 27.5 %copy-start.6 = (bf16[512,128]{1,0:T(8,128)(2,1)S(1)}, bf16[512,128]{1,0:T(8,128)(2,1)}, u32[]{:S(2)}) copy-start(bf16[512,128]{1,0:T(8,128)(2,1)} %param.25) | copy-start | bytes 393220
  41.2 38.1 %copy-start.3 = (bf16[8,64]{1,0:T(8,128)(2,1)S(1)}, bf16[8,64]{1,0:T(8,128)(2,1)}, u32[]{:S(2)}) copy-start(bf16[8,64]{1,0:T(8,128)(2,1)} %param.16) | copy-start | bytes 3076
  41.3 38.1 %copy-start.5 = (bf16[64]{0:T(256)(128)(2,1)S(1)}, bf16[64]{0:T(256)(128)(2,1)}, u32[]{:S(2)}) copy-start(bf16[64]{0:T(256)(128)(2,1)} %param.26) | copy-start | bytes 388
  41.3 42.4 %copy-start.1 = (bf16[128,2816]{1,0:T(8,128)(2,1)S(1)}, bf16[128,2816]{1,0:T(8,128)(2,1)}, u32[]{:S(2)}) copy-start(bf16[128,2816]{1,0:T(8,128)(2,1)} %param.28) | copy-start | bytes 2162692
  41.3 73.9 %copy-start.2 = (bf16[2816,128]{1,0:T(8,128)(2,1)S(1)}, bf16[2816,128]{1,0:T(8,128)(2,1)}, u32[]{:S(2)}) copy-start(bf16[2816,128]{1,0:T(8,128)(2,1)} %param.29) | copy-start | bytes 2162692
  84.5 9.9 %all-to-all-start.5 = ((f32[16,8,1]{1,2,0:T(1,128)}), f32[16,8,1]{1,2,0:T(1,128)S(1)}, u32[]{:S(2)}, u32[]{:S(2)}) async-start(f32[16,8,1]{1,2,0:T(1,128)} %transpose.84), calls=%async_computation.5 | async-start | bytes 16384 | tf_op jit(solution)/shard_map/all_to_all | solution.py:91
  94.4 11.1 %all-to-all-start.4 = ((f32[16,16,176]{2,1,0:T(8,128)}), f32[16,16,176]{2,1,0:T(8,128)S(1)}, u32[]{:S(2)}, u32[]{:S(2)}) async-start(f32[16,16,176]{2,1,0:T(8,128)} %bitcast.224), calls=%async_computation.4 | async-start | bytes 524288 | tf_op jit(solution)/shard_map/all_to_all | solution.py:91
